TPU v7x, 32 devices: a whole 2x2x4 slice. The times are simulated.
32 devices in a mesh: sp: 4 (over z), fs: 4 (over y, x), tp: 2 (over core).
Axes of the slice: x: 2, y: 2, z: 4, core: 2. Of those that a mesh axis runs over, the one named last changes fastest.
Arguments:
- tokens: bfloat16 [12288, 2048], P(('fs', 'sp'), 'tp'), parts along dimension 0, may hold values from -6 to 6
- norm_gain: bfloat16 [2048], replicated, may hold values from 0.099609375 to 1.8984375
- w_query: bfloat16 [2048, 1024], P(None, 'tp'), may hold values from -0.125 to 0.125
- w_key: bfloat16 [2048, 1024], P(None, 'tp'), may hold values from -0.125 to 0.125
- w_value: bfloat16 [2048, 1024], P(None, 'tp'), may hold values from -0.125 to 0.125
- log_decay: float32 [8, 3072], P('tp', 'sp'), may hold values from -1 to 0
- w_conv_in: bfloat16 [2048, 1024], P(None, 'tp'), may hold values from -0.125 to 0.125
- w_conv_pre: bfloat16 [2048, 1024], P(None, 'tp'), may hold values from -0.125 to 0.125
- w_conv_post: bfloat16 [2048, 1024], P(None, 'tp'), may hold values from -0.125 to 0.125
- conv_taps: bfloat16 [3, 1024], P(None, 'tp'), may hold values from -3 to 3
- w_out_ret: bfloat16 [1024, 2048], replicated, may hold values from -0.125 to 0.125
- w_out_conv: bfloat16 [1024, 2048], replicated, may hold values from -0.125 to 0.125
Outputs:
- mixed: bfloat16 [12288, 2048], P(('fs', 'sp', 'tp')), parts along dimension 0
There are 4 independent parts, one for each index of `fs`. A program takes and returns all parts, laid end to end along the dimension named above; an argument that names none is the same for every part. Nothing has to cross between parts.
All inputs are finite; a program needn't handle non-finite values.
Results may differ from a plain program's by a relative error of at most 0.012.
Values may be sent and summed in bfloat16 or wider, within the bound.
A program may use at most 128 MiB of HBM per device.

v0:
```python
import jax
import jax.numpy as jnp
from jax import lax
from jax.sharding import PartitionSpec as P

DH = 128
TAPS = 3
SPAN = 128


epsilon = 1e-06


def shifted(value, axis, steps):
    count = lax.axis_size(axis)
    first, last = (max(0, -steps), min(count, count - steps))
    return lax.ppermute(value, axis, [(source, source + steps) for source in range(first, last)])


def rotate(vectors, positions):
    halfway = vectors.shape[-1] // 2
    inverse = 10000.0 ** (-jnp.arange(halfway, dtype=jnp.float32) / halfway)
    angles = positions.astype(jnp.float32)[:, None] * inverse[None, :]
    cosines = jnp.cos(angles)[:, None, :]
    sinusoid = jnp.sin(angles)[:, None, :]
    leading = vectors[..., :halfway]
    trailing = vectors[..., halfway:]
    return jnp.concatenate(
        [leading * cosines - trailing * sinusoid, leading * sinusoid + trailing * cosines], axis=-1
    )


def body(
    tokens,
    norm_gain,
    w_query,
    w_key,
    w_value,
    log_decay,
    w_conv_in,
    w_conv_pre,
    w_conv_post,
    conv_taps,
    w_out_ret,
    w_out_conv,
):
    gathered = lax.all_gather(tokens, "tp", axis=1, tiled=True)
    floats = gathered.astype(jnp.float32)
    normed = (
        floats
        * lax.rsqrt(jnp.mean(floats * floats, axis=-1, keepdims=True) + epsilon)
        * norm_gain.astype(jnp.float32)
    ).astype(jnp.bfloat16)
    tok_rows = normed.shape[0]
    head_count = w_query.shape[1] // DH
    positions = lax.axis_index("sp") * tok_rows + jnp.arange(tok_rows, dtype=jnp.int32)

    def project(weight):
        return jnp.dot(normed, weight, preferred_element_type=jnp.float32)

    queries = rotate(project(w_query).reshape(tok_rows, head_count, DH), positions).astype(
        jnp.bfloat16
    )
    keys_turned = (
        rotate(project(w_key).reshape(tok_rows, head_count, DH), positions) * DH ** (-0.5)
    ).astype(jnp.bfloat16)
    values = project(w_value).astype(jnp.bfloat16).reshape(tok_rows, head_count, DH)
    conv_in = lax.optimization_barrier(project(w_conv_in).astype(jnp.bfloat16))
    conv_pre = lax.optimization_barrier(project(w_conv_pre).astype(jnp.bfloat16))
    conv_post = lax.optimization_barrier(project(w_conv_post).astype(jnp.bfloat16))
    gated_in = (conv_pre.astype(jnp.float32) * conv_in.astype(jnp.float32)).astype(jnp.bfloat16)
    rim_rows = shifted(gated_in[tok_rows - (TAPS - 1) :], "sp", 1)
    extended = jnp.concatenate([rim_rows, gated_in], axis=0)
    convolved = jnp.zeros(gated_in.shape, jnp.float32)
    for tap_index in range(TAPS):
        convolved = convolved + conv_taps[tap_index].astype(jnp.float32) * extended[
            tap_index : tap_index + tok_rows
        ].astype(jnp.float32)
    conv_out = (conv_post.astype(jnp.float32) * convolved).astype(jnp.bfloat16)
    blocks = tok_rows // SPAN
    query_blocks = queries.reshape(blocks, SPAN, head_count, DH)
    key_blocks = keys_turned.reshape(blocks, SPAN, head_count, DH)
    value_blocks = values.reshape(blocks, SPAN, head_count, DH)
    cumulative = jnp.cumsum(log_decay.reshape(head_count, blocks, SPAN), axis=-1).transpose(1, 0, 2)
    lower_mask = jnp.tril(jnp.ones((SPAN, SPAN), bool))
    differences = cumulative[..., :, None] - cumulative[..., None, :]
    decay_weights = jnp.where(lower_mask, jnp.exp(jnp.minimum(differences, 0.0)), 0.0)
    scores = jnp.einsum(
        "bshd,bthd->bhst", query_blocks, key_blocks, preferred_element_type=jnp.float32
    )
    mix_weights = (scores * decay_weights).astype(jnp.bfloat16)
    inside = jnp.einsum(
        "bhst,bthd->bshd", mix_weights, value_blocks, preferred_element_type=jnp.float32
    )
    block_ends = cumulative[..., -1]
    tail_decay = jnp.exp(block_ends[..., None] - cumulative)
    weighted = value_blocks.astype(jnp.float32) * tail_decay.transpose(0, 2, 1)[..., None]
    block_states = jnp.einsum(
        "bshd,bshe->bhde", key_blocks.astype(jnp.float32), weighted, precision=lax.Precision.HIGHEST
    )

    def advance(carried, inputs):
        end_decay, fresh_state = inputs
        return (jnp.exp(end_decay)[:, None, None] * carried + fresh_state, carried)

    empty_state = jnp.zeros((head_count, DH, DH), jnp.float32)
    local_total, local_starts = lax.scan(advance, empty_state, (block_ends, block_states))
    decay_total = jnp.exp(jnp.sum(block_ends, axis=0))
    all_decays, all_states = (
        lax.all_gather(decay_total[None].astype(jnp.bfloat16), "sp", axis=0, tiled=True).astype(
            jnp.float32
        ),
        lax.all_gather(local_total[None].astype(jnp.bfloat16), "sp", axis=0, tiled=True).astype(
            jnp.float32
        ),
    )
    position_index = lax.axis_index("sp")

    def absorb(source, carried):
        absorbed = all_decays[source][:, None, None] * carried + all_states[source]
        return jnp.where(source < position_index, absorbed, carried)

    incoming = lax.fori_loop(0, lax.axis_size("sp"), absorb, empty_state)
    prefix_ends = jnp.cumsum(block_ends, axis=0) - block_ends
    starts = local_starts + jnp.exp(prefix_ends)[..., None, None] * incoming[None]
    across = jnp.einsum(
        "bshd,bhde->bshe", query_blocks.astype(jnp.float32), starts, precision=lax.Precision.HIGHEST
    )
    retained = inside + jnp.exp(cumulative).transpose(0, 2, 1)[..., None] * across
    normalized = retained * lax.rsqrt(
        jnp.mean(retained * retained, axis=-1, keepdims=True) + epsilon
    )
    ret_out = normalized.astype(jnp.bfloat16).reshape(tok_rows, head_count * DH)
    ret_width = ret_out.shape[1]
    conv_width = conv_out.shape[1]
    pair_index = lax.axis_index("tp")
    ret_rows = lax.dynamic_slice_in_dim(w_out_ret, pair_index * ret_width, ret_width, 0)
    conv_rows = lax.dynamic_slice_in_dim(w_out_conv, pair_index * conv_width, conv_width, 0)
    return lax.psum_scatter(
        (
            jnp.dot(ret_out, ret_rows, preferred_element_type=jnp.float32)
            + jnp.dot(conv_out, conv_rows, preferred_element_type=jnp.float32)
        ).astype(jnp.bfloat16),
        "tp",
        scatter_dimension=0,
        tiled=True,
    )


def solution(mesh):
    in_specs = (
        P(("fs", "sp"), "tp"),
        P(),
        P(None, "tp"),
        P(None, "tp"),
        P(None, "tp"),
        P("tp", "sp"),
        P(None, "tp"),
        P(None, "tp"),
        P(None, "tp"),
        P(None, "tp"),
        P(),
        P(),
    )
    out_specs = P(("fs", "sp", "tp"), None)
    return jax.shard_map(body, mesh=mesh, in_specs=in_specs, out_specs=out_specs, check_vma=False)
```

profile of v0, /device:TPU:21, one launch (start us, length us, event | category | flops | bytes accessed | tf_op | source)
XLA Modules:
  0.0 140.2 jit_solution(10205250472383561693)
XLA Ops:
  11.5 7.0 %all-reduce = bf16[16]{0:T(256)(128)(2,1)S(1)} all-reduce(bf16[16]{0:T(256)(128)(2,1)S(1)} %dynamic-update-slice), channel_id=2, replica_groups=mesh['sp'=4,'fs'=4,'tp'=2] {'sp'}, use_global_device_ids=true, to_apply=%add | all-reduce | flops 16 | bytes 64
  22.8 2.7 %fusion.3 = f32[768]{0:T(1024)S(1)} fusion(bf16[768,2048]{1,0:T(8,128)(2,1)} %all-gather.4.cloned.1.call-done), kind=kLoop, calls=%fused_computation.10 | loop fusion | flops 4717824 | bytes 3148800 | tf_op jit(solution)/shard_map/reduce_sum | solution.py:51
  25.6 1.8 %convolution_convert_fusion.1 = bf16[768,512]{1,0:T(8,128)(2,1)S(1)} fusion(bf16[2048,512]{1,0:T(8,128)(2,1)S(1)} %copy-done, bf16[768,2048]{1,0:T(8,128)(2,1)S(1)} %copy-done.1, f32[2048]{0:T(1024)S(1)} %convert_element_type.106, f32[768]{0:T(1024)S(1)} %add_rsqrt_fusion.1), kind=kOutput, calls=%fused_computation.33 | convolution fusion | flops 1617297408 | bytes 6040576 | tf_op jit(solution)/shard_map/dot_general | solution.py:59
  30.4 3.3 %collective-permute-start = (bf16[2,512]{1,0:T(2,128)(2,1)S(1)}, bf16[2,512]{1,0:T(2,128)(2,1)S(1)}, u32[]{:S(2)}, u32[]{:S(2)}) collective-permute-start(bf16[2,512]{1,0:T(2,128)(2,1)S(1)} %slice.49), channel_id=1, source_target_pairs={{0,8},{8,16},{16,24},{1,9},{9,17},{17,25},{2,10},{10,18},{18,26},{... | collective-permute-start | bytes 6152 | tf_op jit(solution)/shard_map/ppermute | solution.py:17
  33.7 2.7 %convolution_convert_fusion.3 = bf16[768,512]{1,0:T(8,128)(2,1)} fusion(bf16[2048,512]{1,0:T(8,128)(2,1)S(1)} %copy-done.13, bf16[768,2048]{1,0:T(8,128)(2,1)S(1)} %copy-done.1, f32[2048]{0:T(1024)S(1)} %convert_element_type.106, f32[768]{0:T(1024)S(1)} %add_rsqrt_fusion.1), kind=kOutput, calls=%fused_computation.35 | convolution fusion | flops 1617297408 | bytes 6040576 | tf_op jit(solution)/shard_map/dot_general | solution.py:59
  38.2 4.9 %fusion.49 = f32[768,512]{0,1:T(8,128)S(1)} fusion(bf16[2048,512]{1,0:T(8,128)(2,1)} %param.18, bf16[768,2048]{1,0:T(8,128)(2,1)} %all-gather.4.cloned.1.call-done, f32[2048]{0:T(1024)S(1)} %convert_element_type.106, f32[768]{0:T(1024)S(1)} %add_rsqrt_fusion.1), kind=kOutput, calls=%fused_computation.85 | convolution fusion | flops 1616904192 | bytes 6827008 | tf_op jit(solution)/shard_map/dot_general | solution.py:59
  43.2 2.0 %fusion.47 = f32[768,512]{0,1:T(8,128)S(1)} fusion(bf16[2048,512]{1,0:T(8,128)(2,1)S(1)} %copy-done.14, bf16[768,2048]{1,0:T(8,128)(2,1)S(1)} %copy-done.2, f32[2048]{0:T(1024)S(1)} %convert_element_type.106, f32[768]{0:T(1024)S(1)} %add_rsqrt_fusion.1), kind=kOutput, calls=%fused_computation.84 | convolution fusion | flops 1616904192 | bytes 6827008 | tf_op jit(solution)/shard_map/dot_general | solution.py:59
  46.9 2.3 %concatenate.20 = bf16[6,128,4,64]{1,0,3,2:T(8,128)(2,1)} reshape(bf16[768,4,64]{0,2,1:T(8,128)(2,1)} %get-tuple-element.203) | data formatting | bytes 786432 | tf_op jit(solution)/shard_map/concatenate | solution.py:28
  49.2 2.3 %copy.36 = bf16[6,128,4,64]{3,1,2,0:T(8,128)(2,1)} copy(bf16[6,128,4,64]{1,0,3,2:T(8,128)(2,1)} %concatenate.20) | data formatting | bytes 786432 | tf_op jit(solution)/shard_map/concatenate | solution.py:28
  51.5 2.2 %concatenate.21 = bf16[6,128,4,64]{1,0,3,2:T(8,128)(2,1)} reshape(bf16[768,4,64]{0,2,1:T(8,128)(2,1)} %get-tuple-element.204) | data formatting | bytes 786432 | tf_op jit(solution)/shard_map/concatenate | solution.py:28
  53.8 2.3 %copy.37 = bf16[6,128,4,64]{3,1,2,0:T(8,128)(2,1)} copy(bf16[6,128,4,64]{1,0,3,2:T(8,128)(2,1)} %concatenate.21) | data formatting | bytes 786432 | tf_op jit(solution)/shard_map/concatenate | solution.py:28
  56.1 2.3 %concatenate.24 = f32[6,128,4,64]{1,0,3,2:T(8,128)} reshape(f32[768,4,64]{0,2,1:T(8,128)} %get-tuple-element.207) | data formatting | bytes 1572864 | tf_op jit(solution)/shard_map/concatenate | solution.py:28
  58.3 2.9 %copy.39 = f32[6,128,4,64]{3,1,2,0:T(8,128)} copy(f32[6,128,4,64]{1,0,3,2:T(8,128)} %concatenate.24) | data formatting | bytes 1572864 | tf_op jit(solution)/shard_map/concatenate | solution.py:28
  61.2 2.3 %concatenate.23 = f32[6,128,4,64]{1,0,3,2:T(8,128)} reshape(f32[768,4,64]{0,2,1:T(8,128)} %get-tuple-element.208) | data formatting | bytes 1572864 | tf_op jit(solution)/shard_map/concatenate | solution.py:28
  63.4 2.9 %copy.38 = f32[6,128,4,64]{3,1,2,0:T(8,128)} copy(f32[6,128,4,64]{1,0,3,2:T(8,128)} %concatenate.23) | data formatting | bytes 1572864 | tf_op jit(solution)/shard_map/concatenate | solution.py:28
  66.3 2.4 %fusion.9 = bf16[6,128,4,128]{3,1,2,0:T(8,128)(2,1)S(1)} fusion(f32[6,128,4,64]{3,1,2,0:T(8,128)} %copy.39, f32[6,128,4,64]{3,1,2,0:T(8,128)} %copy.38), kind=kLoop, calls=%fused_computation.18 | loop fusion | flops 1179648 | bytes 2359296 | tf_op jit(solution)/shard_map/convert_element_type | solution.py:66
  68.7 2.6 %fusion.14 = f32[6,4,128,128]{3,2,1,0:T(8,128)} fusion(bf16[6,128,4,128]{3,1,2,0:T(8,128)(2,1)S(1)} %fusion.9, f32[6,128,4]{1,2,0:T(4,128)S(1)} %copy.45, bf16[6,128,4,128]{3,2,1,0:T(4,128)(2,1)S(1)} %reshape_reshape.3), kind=kOutput, calls=%fused_computation.28 | convolution fusion | flops 604766208 | bytes 3158016 | tf_op jit(solution)/shard_map/bshd,bshe->bhde/dot_general | solution.py:98
  71.3 10.8 %while.29 = (s32[]{:T(128)}, f32[4,128,128]{2,1,0:T(8,128)S(1)}, f32[6,4,128,128]{3,2,1,0:T(8,128)}, f32[6,4]{1,0:T(8,128)S(1)}, f32[6,4,128,128]{3,2,1,0:T(8,128)}) while((s32[]{:T(128)}, f32[4,128,128]{2,1,0:T(8,128)S(1)}, f32[6,4,128,128]{3,2,1,0:T(8,128)}, f32[6,4]{1,0:T(8,128)S(1)}, ...), condition=%wide.region_3.4_spmd.clone.clone, body=%wide.region_2.3_spmd.clone.sunk.clone | while | flops 262147 | bytes 1310860 | solution.py:107
  82.1 12.3 %all-gather.1 = bf16[16,128,128]{2,1,0:T(8,128)(2,1)S(1)} all-gather(bf16[4,128,128]{2,1,0:T(8,128)(2,1)S(1)} %convert_element_type.116), channel_id=3, replica_groups=mesh['sp'=4,'fs'=4,'tp'=2] {'sp'}, dimensions={0}, use_global_device_ids=true | all-gather | bytes 655360 | tf_op jit(solution)/shard_map/all_gather | solution.py:113
  95.1 4.3 %fusion.19 = f32[6,4,128,128]{3,2,1,0:T(8,128)} fusion(bf16[6,128,4,128]{3,1,2,0:T(8,128)(2,1)} %copy-done.5, f32[6,4,128]{2,1,0:T(4,128)S(1)} %copy.40, pred[128,128]{1,0:T(8,128)(4,1)S(1)} %iota_compare_fusion, bf16[6,128,4,128]{3,2,1,0:T(4,128)(2,1)} %copy-done.3, bf16[6,128,4,64]{3,1,2,0:T(8,128)(2,1)} %copy.37, bf16[6,128,4,64]{3,1,2,0:T(8,128)(2,1)} %copy.36), kind=kOutput, calls=%fused_computation.36 | convolution fusion | flops 204865536 | bytes 3960832 | tf_op jit(solution)/shard_map/bhst,bthd->bshd/dot_general | solution.py:92
  99.5 3.9 %multiply_reduce_fusion = (f32[6,128,4]{1,2,0:T(4,128)S(1)}, f32[6,128,4,128]{1,3,2,0:T(8,128)S(1)}) fusion(bf16[6,128,4,64]{3,1,2,0:T(8,128)(2,1)} %copy.37, bf16[6,128,4,64]{3,1,2,0:T(8,128)(2,1)S(1)} %copy-done.4, f32[6,4,128,128]{3,2,1,0:T(8,128)} %get-tuple-element.127, f32[4,128,128]{2,1,0:T(8,128)S(1)} %get-tuple-element.129, f32[6,4]{1,0:T(8,128)S(1)} %copy.48, ...), kind=kOutput, calls=%fused_computation.24 | convolution fusion | flops 607908864 | bytes 5791840 | tf_op jit(solution)/shard_map/bshd,bhde->bshe/dot_general | solution.py:126
  106.0 4.5 %convolution_convert_fusion.2 = bf16[768,512]{1,0:T(8,128)(2,1)S(1)} fusion(bf16[2048,512]{1,0:T(8,128)(2,1)} %param.24, bf16[768,2048]{1,0:T(8,128)(2,1)} %all-gather.4.cloned.1.call-done, f32[2048]{0:T(1024)S(1)} %convert_element_type.106, f32[768]{0:T(1024)S(1)} %add_rsqrt_fusion.1), kind=kOutput, calls=%fused_computation.34 | convolution fusion | flops 1617297408 | bytes 6040576 | tf_op jit(solution)/shard_map/dot_general | solution.py:59
  113.0 3.8 %add_convert_fusion = bf16[768,2048]{1,0:T(8,128)(2,1)} fusion(f32[768,2048]{1,0:T(8,128)S(1)} %fusion.7, bf16[1024,2048]{1,0:T(8,128)(2,1)S(1)} %copy-done.11, s32[]{:T(128)S(6)} %select_n.33, bf16[768,512]{1,0:T(8,128)(2,1)S(1)} %copy-done.8, bf16[768,512]{1,0:T(8,128)(2,1)S(1)} %convolution_convert_fusion.2, ...), kind=kOutput, calls=%fused_computation.13 | convolution fusion | flops 1620443136 | bytes 13115396 | tf_op jit(solution)/shard_map/dot_general | solution.py:142
  116.9 16.5 %reduce-scatter.2.cloned.1.call-done = bf16[384,2048]{1,0:T(8,128)(2,1)} async-done(((bf16[768,2048]{1,0:T(8,128)(2,1)}), bf16[384,2048]{1,0:T(8,128)(2,1)}) %reduce-scatter.2.cloned.1.call-update) | async-done | bytes 1572880 | tf_op jit(solution)/shard_map/reduce_scatter | solution.py:139
  (100 shorter events, 31.9 us)
Async XLA Ops:
  6.5 19.0 %copy-start = (bf16[2048,512]{1,0:T(8,128)(2,1)S(1)}, bf16[2048,512]{1,0:T(8,128)(2,1)}, u32[]{:S(2)}) copy-start(bf16[2048,512]{1,0:T(8,128)(2,1)} %param.23) | copy-start | bytes 6291460
  6.5 16.2 %all-gather.4.cloned.1.call-start = ((), (), s32[]{:S(2)}) async-start(), calls=%async_computation.1 | async-start | bytes 4718592 | tf_op jit(solution)/shard_map/all_gather | solution.py:47
  7.3 126.1 %reduce-scatter.2.cloned.1.call-start = ((), (), s32[]{:S(2)}) async-start(), calls=%async_computation.2 | async-start | bytes 4718592 | tf_op jit(solution)/shard_map/reduce_scatter | solution.py:139
  22.8 2.8 %copy-start.1 = (bf16[768,2048]{1,0:T(8,128)(2,1)S(1)}, bf16[768,2048]{1,0:T(8,128)(2,1)}, u32[]{:S(2)}) copy-start(bf16[768,2048]{1,0:T(8,128)(2,1)} %all-gather.4.cloned.1.call-done) | copy-start | bytes 9437188
  25.6 1.9 %copy-start.12 = (bf16[2048,512]{1,0:T(8,128)(2,1)S(1)}, bf16[2048,512]{1,0:T(8,128)(2,1)}, u32[]{:S(2)}) copy-start(bf16[2048,512]{1,0:T(8,128)(2,1)} %param.22) | copy-start | bytes 6291460
  29.3 4.4 %copy-start.13 = (bf16[2048,512]{1,0:T(8,128)(2,1)S(1)}, bf16[2048,512]{1,0:T(8,128)(2,1)}, u32[]{:S(2)}) copy-start(bf16[2048,512]{1,0:T(8,128)(2,1)} %param.20) | copy-start | bytes 6291460
  29.5 0.9 copy-start.7
  30.4 82.0 %collective-permute-start = (bf16[2,512]{1,0:T(2,128)(2,1)S(1)}, bf16[2,512]{1,0:T(2,128)(2,1)S(1)}, u32[]{:S(2)}, u32[]{:S(2)}) collective-permute-start(bf16[2,512]{1,0:T(2,128)(2,1)S(1)} %slice.49), channel_id=1, source_target_pairs={{0,8},{8,16},{16,24},{1,9},{9,17},{17,25},{2,10},{10,18},{18,26},{... | collective-permute-start | bytes 6152 | tf_op jit(solution)/shard_map/ppermute | solution.py:17
  38.2 30.4 %copy-start.3 = (bf16[6,128,4,128]{3,2,1,0:T(4,128)(2,1)}, bf16[6,128,4,128]{3,2,1,0:T(4,128)(2,1)S(1)}, u32[]{:S(2)}) copy-start(bf16[6,128,4,128]{3,2,1,0:T(4,128)(2,1)S(1)} %reshape_reshape.3) | copy-start | bytes 2359300
  38.2 4.9 %copy-start.2 = (bf16[768,2048]{1,0:T(8,128)(2,1)S(1)}, bf16[768,2048]{1,0:T(8,128)(2,1)}, u32[]{:S(2)}) copy-start(bf16[768,2048]{1,0:T(8,128)(2,1)} %all-gather.4.cloned.1.call-done) | copy-start | bytes 9437188
  38.2 4.9 %copy-start.14 = (bf16[2048,512]{1,0:T(8,128)(2,1)S(1)}, bf16[2048,512]{1,0:T(8,128)(2,1)}, u32[]{:S(2)}) copy-start(bf16[2048,512]{1,0:T(8,128)(2,1)} %param.19) | copy-start | bytes 6291460
  43.1 2.1 %copy-start.9 = (f32[768,64]{0,1:T(8,128)S(1)}, f32[768,64]{0,1:T(8,128)}, u32[]{:S(2)}) copy-start(f32[768,64]{0,1:T(8,128)} %get-tuple-element.211) | copy-start | bytes 589828
  43.2 2.1 %copy-start.10 = (f32[768,64]{0,1:T(8,128)S(1)}, f32[768,64]{0,1:T(8,128)}, u32[]{:S(2)}) copy-start(f32[768,64]{0,1:T(8,128)} %get-tuple-element.212) | copy-start | bytes 589828
  68.7 2.6 %copy-start.5 = (bf16[6,128,4,128]{3,1,2,0:T(8,128)(2,1)}, bf16[6,128,4,128]{3,1,2,0:T(8,128)(2,1)S(1)}, u32[]{:S(2)}) copy-start(bf16[6,128,4,128]{3,1,2,0:T(8,128)(2,1)S(1)} %fusion.9) | copy-start | bytes 2359300
  95.1 4.3 %copy-start.4 = (bf16[6,128,4,64]{3,1,2,0:T(8,128)(2,1)S(1)}, bf16[6,128,4,64]{3,1,2,0:T(8,128)(2,1)}, u32[]{:S(2)}) copy-start(bf16[6,128,4,64]{3,1,2,0:T(8,128)(2,1)} %copy.36) | copy-start | bytes 1179652
  106.0 4.6 %copy-start.6 = (bf16[1024,2048]{1,0:T(8,128)(2,1)S(1)}, bf16[1024,2048]{1,0:T(8,128)(2,1)}, u32[]{:S(2)}) copy-start(bf16[1024,2048]{1,0:T(8,128)(2,1)} %param.26) | copy-start | bytes 12582916
  110.6 1.9 %copy-start.8 = (bf16[768,512]{1,0:T(8,128)(2,1)S(1)}, bf16[768,512]{1,0:T(8,128)(2,1)}, u32[]{:S(2)}) copy-start(bf16[768,512]{1,0:T(8,128)(2,1)} %copy-done.7) | copy-start | bytes 2359300
  110.6 2.4 %copy-start.11 = (bf16[1024,2048]{1,0:T(8,128)(2,1)S(1)}, bf16[1024,2048]{1,0:T(8,128)(2,1)}, u32[]{:S(2)}) copy-start(bf16[1024,2048]{1,0:T(8,128)(2,1)} %param.27) | copy-start | bytes 12582916
Sparse Core Ops, SparseCore 0:
  8.9 13.8 all-gather.3
  117.0 16.2 reduce-scatter.1
where the time goes:
time: 142 us; the launch traced here: 140 us
  matrix products  34.4 us (24%)
  local copies, waits for them, and re-layouts  26.8 us (19%)
  other arithmetic  23.9 us (17%)
  blocking collectives  19.3 us (14%)
  waiting for transfers between devices  17.9 us (13%)
  between operations  14.4 us (10%)
  starting transfers between devices  3.32 us (2%)
    concatenate x8, local copies, waits for them, and re-layouts, rotate(): jnp.concatenate([leading * cosines - trailing * sinusoid, leading * sinus...  19.3 us
    dot_general x6, matrix products, project(): return jnp.dot(normed, weight, preferred_element_type=jnp.float32)  17.8 us
    reduce_scatter x1, waiting for transfers between devices, body(): lax.psum_scatter((jnp.dot(ret_out, ret_rows, preferred_element_type=jnp.f...  16.5 us
    all_gather x1, blocking collectives, body(): lax.all_gather(local_total[None].astype(jnp.bfloat16), 'sp', axis=0, tile...  12.3 us
    unnamed x1, blocking collectives  6.95 us
    add x6, other arithmetic, advance(): return (jnp.exp(end_decay)[:, None, None] * carried + fresh_state, carried)  6.24 us
    dynamic_update_slice x6, other arithmetic, body(): lax.scan(advance, empty_state, (block_ends, block_states))  4.36 us
    dot_general x1, matrix products, body(): jnp.einsum('bhst,bthd->bshd', mix_weights, value_blocks, preferred_elemen...  4.33 us
  transfers between devices with their start and end apart: 3, of which 2 were waited for; matrix products, arithmetic and copies ran while one was open for 52% of the time, Pallas kernels for 0%

commit v1 on v0

v1 whole, which is shorter than its diff:
```python
import functools

import jax
import jax.numpy as jnp
import numpy as np
from jax import lax
from jax.experimental import pallas as pl
from jax.experimental.pallas import tpu as pltpu
from jax.sharding import PartitionSpec as P

DH = 128
TAPS = 3
SPAN = 128
EPSILON = 1e-06
BF = jnp.bfloat16
F32 = jnp.float32


def dot(a, b, dims=((1,), (0,)), precision=None):
    return lax.dot_general(
        a, b, (dims, ((), ())), preferred_element_type=F32, precision=precision
    )


def kernel(
    sp_count,
    tok_hbm,
    gain_hbm,
    wq_hbm,
    wk_hbm,
    wv_hbm,
    decay_hbm,
    win_hbm,
    wpre_hbm,
    wpost_hbm,
    taps_hbm,
    wor_hbm,
    woc_hbm,
    inner_hbm,
    outer_hbm,
    out_hbm,
    tok,
    normed,
    weights,
    w_ret,
    w_conv,
    gain,
    decay,
    taps,
    inner,
    outer,
    rope_c,
    rope_s,
    cum_row,
    cum_col,
    exp_col,
    tail_col,
    queries,
    keys,
    values,
    post,
    gated,
    starts,
    running,
    state_out,
    state_in,
    incoming,
    inside,
    conv_all,
    conv_in,
    ret_all,
    ret_in,
    total,
    out_vmem,
    load_sem,
    tok_send,
    tok_recv,
    tok_load,
    state_send,
    state_recv,
    pair_send,
    pair_recv,
    rim_send,
    rim_recv,
    out_sem,
):
    rows, half_width = tok_hbm.shape
    width = 2 * half_width
    heads = decay_hbm.shape[0]
    blocks = rows // SPAN
    half = rows // 2
    half_blocks = blocks // 2
    local = heads * DH
    sp = lax.axis_index("sp")
    tp = lax.axis_index("tp")
    other = 1 - tp

    loads = [
        (gain_hbm, gain),
        (decay_hbm, decay),
        (taps_hbm, taps),
        (inner_hbm, inner),
        (outer_hbm.at[sp], outer),
        (wk_hbm, weights.at[0]),
        (wv_hbm, weights.at[1]),
        (wq_hbm, weights.at[2]),
        (win_hbm, weights.at[3]),
        (wpre_hbm, weights.at[4]),
        (wpost_hbm, weights.at[5]),
        (woc_hbm, w_conv),
        (wor_hbm, w_ret),
    ]
    loads = [
        pltpu.make_async_copy(source, target, load_sem.at[i])
        for i, (source, target) in enumerate(loads)
    ]
    (l_gain, l_decay, l_taps, l_inner, l_outer) = loads[:5]
    l_weights = loads[5:11]
    l_woc, l_wor = loads[11:]

    barrier = pltpu.get_barrier_semaphore()
    pl.semaphore_signal(barrier, inc=1, device_id={"tp": other})
    for step in range(1, sp_count):
        pl.semaphore_signal(barrier, inc=1, device_id={"sp": lax.rem(sp + step, sp_count)})

    chunk_rows = [pl.ds(c * half, half) for c in range(2)]
    own_copies = [
        pltpu.make_async_copy(tok_hbm.at[r], tok.at[tp, r], tok_load.at[c])
        for c, r in enumerate(chunk_rows)
    ]
    for copy in loads[:5]:
        copy.start()
    own_copies[0].start()
    own_copies[1].start()
    l_weights[0].start()
    l_weights[1].start()
    pl.semaphore_wait(barrier, sp_count)
    tok_copies = [
        pltpu.make_async_remote_copy(
            src_ref=tok_hbm.at[r],
            dst_ref=tok.at[tp, r],
            send_sem=tok_send.at[c],
            recv_sem=tok_recv.at[c],
            device_id={"tp": other},
        )
        for c, r in enumerate(chunk_rows)
    ]
    for copy in tok_copies:
        copy.start()
    for copy in l_weights[2:]:
        copy.start()
    l_woc.start()
    l_wor.start()

    l_inner.wait()
    l_outer.wait()
    l_decay.wait()
    l_gain.wait()
    row_id = lax.broadcasted_iota(jnp.int32, (SPAN, SPAN), 0)
    col_id = lax.broadcasted_iota(jnp.int32, (SPAN, SPAN), 1)
    lower = row_id >= col_id
    lower_f = jnp.where(lower, 1.0, 0.0)
    for b in range(blocks):
        at = slice(b * SPAN, (b + 1) * SPAN)
        cos_b = outer[0, b : b + 1, :]
        sin_b = outer[1, b : b + 1, :]
        rope_c[at, :] = inner[0] * cos_b - inner[1] * sin_b
        rope_s[at, :] = inner[1] * cos_b + inner[0] * sin_b
        logs = decay[:, at]
        by_row = dot(logs, lower_f, ((1,), (1,)), lax.Precision.HIGHEST)
        by_col = dot(lower_f, logs, ((1,), (1,)), lax.Precision.HIGHEST)
        cum_row[b] = by_row
        cum_col[at, :] = by_col
        exp_col[at, :] = jnp.exp(by_col)
        tail_col[at, :] = jnp.exp(by_col[SPAN - 1 : SPAN, :] - by_col)
    running[...] = jnp.zeros_like(running)
    incoming[...] = jnp.zeros_like(incoming)

    def norm_chunk(c):
        def step(i, _):
            at = pl.ds(pl.multiple_of(c * half + i * 32, 32), 32)
            x0 = tok[0, at, :].astype(F32)
            x1 = tok[1, at, :].astype(F32)
            squares = jnp.sum(x0 * x0 + x1 * x1, axis=-1, keepdims=True)
            scale = lax.rsqrt(squares * (1.0 / width) + EPSILON)
            normed[at, :half_width] = (x0 * scale * gain[:, :half_width].astype(F32)).astype(BF)
            normed[at, half_width:] = (x1 * scale * gain[:, half_width:].astype(F32)).astype(BF)
            return 0

        lax.fori_loop(0, half // 32, step, 0)

    def project(c, which):
        return dot(normed[c * half : (c + 1) * half, :], weights[which])

    def rotate_into(target, product, c, factor):
        for b in range(half_blocks):
            at = slice(c * half + b * SPAN, c * half + (b + 1) * SPAN)
            cosines = rope_c[at, :]
            sines = rope_s[at, :]
            if factor is not None:
                cosines = cosines * factor
                sines = sines * factor
            for h in range(heads):
                x = product[b * SPAN : (b + 1) * SPAN, h * DH : (h + 1) * DH]
                turned = x * cosines + pltpu.roll(x, DH // 2, 1) * sines
                target[at, h * DH : (h + 1) * DH] = turned.astype(BF)

    for c in range(2):
        own_copies[c].wait()
        tok_copies[c].wait_recv()
        norm_chunk(c)
        if c == 0:
            l_weights[0].wait()
            l_weights[1].wait()
        rotate_into(keys, project(c, 0), c, DH**-0.5)
        values[c * half : (c + 1) * half, :] = project(c, 1).astype(BF)

    def state_step(b, _):
        at = pl.ds(pl.multiple_of(b * SPAN, SPAN), SPAN)
        ends = jnp.exp(cum_row[b][:, SPAN - 1 : SPAN])
        for h in range(heads):
            cols = slice(h * DH, (h + 1) * DH)
            weighted = (values[at, cols].astype(F32) * tail_col[at, h : h + 1]).astype(BF)
            fresh = dot(keys[at, cols], weighted, ((0,), (0,)))
            held = running[cols, :]
            starts[b, cols, :] = held
            running[cols, :] = ends[h : h + 1, :] * held + fresh
        return 0

    lax.fori_loop(0, blocks, state_step, 0)
    state_out[0:local, :] = running[...].astype(BF)
    ends_total = cum_row[0][:, SPAN - 1 : SPAN]
    for b in range(1, blocks):
        ends_total = ends_total + cum_row[b][:, SPAN - 1 : SPAN]
    for h in range(heads):
        state_out[local + 16 * h : local + 16 * (h + 1), :] = jnp.broadcast_to(
            jnp.exp(ends_total[h : h + 1, :]), (16, DH)
        ).astype(BF)

    l_weights[2].wait()
    rotate_into(queries, project(0, 2), 0, None)

    def state_copy(step):
        return pltpu.make_async_remote_copy(
            src_ref=state_out,
            dst_ref=state_in.at[step - 1],
            send_sem=state_send.at[step - 1],
            recv_sem=state_recv.at[step - 1],
            device_id={"sp": lax.rem(sp + step, sp_count)},
        )

    for step in range(1, sp_count):
        @pl.when(sp + step < sp_count)
        def _():
            state_copy(step).start()

    rotate_into(queries, project(1, 2), 1, None)

    l_weights[3].wait()
    l_weights[4].wait()
    for c in range(2):
        first = project(c, 3).astype(BF).astype(F32)
        second = project(c, 4).astype(BF).astype(F32)
        gated[8 + c * half : 8 + (c + 1) * half, :] = (first * second).astype(BF).astype(F32)

    @pl.when(sp == 0)
    def _():
        gated[0:8, :] = jnp.zeros((8, local), F32)

    l_weights[5].wait()
    post[0:half, :] = project(0, 5).astype(BF)
    rim_copy = pltpu.make_async_remote_copy(
        src_ref=gated.at[pl.ds(rows, 8)],
        dst_ref=gated.at[pl.ds(0, 8)],
        send_sem=rim_send,
        recv_sem=rim_recv,
        device_id={"sp": lax.rem(sp + 1, sp_count)},
    )

    @pl.when(sp + 1 < sp_count)
    def _():
        rim_copy.start()

    post[half:, :] = project(1, 5).astype(BF)

    def inside_step(b, _):
        at = pl.ds(pl.multiple_of(b * SPAN, SPAN), SPAN)
        row = cum_row[b]
        for h in range(heads):
            cols = slice(h * DH, (h + 1) * DH)
            scores = dot(queries[at, cols], keys[at, cols], ((1,), (1,)))
            gap = jnp.minimum(cum_col[at, h : h + 1] - row[h : h + 1, :], 0.0)
            mix = (scores * jnp.where(lower, jnp.exp(gap), 0.0)).astype(BF)
            inside[at, cols] = dot(mix, values[at, cols])
        return 0

    lax.fori_loop(0, blocks, inside_step, 0)

    @pl.when(sp > 0)
    def _():
        rim_copy.wait_recv()

    l_taps.wait()
    tap = [taps[i : i + 1, :].astype(F32) for i in range(TAPS)]
    for b in range(blocks):
        base = b * SPAN + 8 - (TAPS - 1)
        convolved = tap[0] * gated[base : base + SPAN, :]
        for i in range(1, TAPS):
            convolved = convolved + tap[i] * gated[base + i : base + i + SPAN, :]
        at = slice(b * SPAN, (b + 1) * SPAN)
        conv_all[at, :] = (post[at, :].astype(F32) * convolved).astype(BF)

    def pair_copy(source, target, i):
        return pltpu.make_async_remote_copy(
            src_ref=source.at[pl.ds(pl.multiple_of(other * half, half), half)],
            dst_ref=target,
            send_sem=pair_send.at[i],
            recv_sem=pair_recv.at[i],
            device_id={"tp": other},
        )

    mine = pl.ds(pl.multiple_of(tp * half, half), half)
    my_inputs = pl.ds(pl.multiple_of(tp * local, local), local)
    other_inputs = pl.ds(pl.multiple_of(other * local, local), local)
    tiles = width // 512

    def tile_at(n):
        return pl.ds(pl.multiple_of(n * 512, 512), 512)

    l_woc.wait()
    conv_copy = pair_copy(conv_all, conv_in, 0)
    conv_copy.start()

    def conv_own(n, _):
        total[:, tile_at(n)] = dot(conv_all[mine, :], w_conv[my_inputs, tile_at(n)])
        return 0

    lax.fori_loop(0, tiles, conv_own, 0)
    conv_copy.wait_recv()

    def conv_other(n, _):
        total[:, tile_at(n)] += dot(conv_in[...], w_conv[other_inputs, tile_at(n)])
        return 0

    lax.fori_loop(0, tiles, conv_other, 0)

    for step in range(sp_count - 1, 0, -1):
        @pl.when(sp >= step)
        def _():
            state_copy(step).wait_recv()
            for h in range(heads):
                cols = slice(h * DH, (h + 1) * DH)
                shrink = state_in[step - 1, local + 16 * h : local + 16 * (h + 1), :].astype(F32)
                incoming[cols, :] = (
                    shrink[0:1, :] * incoming[cols, :] + state_in[step - 1, cols, :].astype(F32)
                )

    def across_half(which):
        def step(i, before):
            b = which * half_blocks + i
            at = pl.ds(pl.multiple_of(b * SPAN, SPAN), SPAN)
            factor = jnp.exp(before)
            for h in range(heads):
                cols = slice(h * DH, (h + 1) * DH)
                state = (starts[b, cols, :] + factor[h : h + 1, :] * incoming[cols, :]).astype(BF)
                across = dot(queries[at, cols], state)
                retained = inside[at, cols] + exp_col[at, h : h + 1] * across
                power = jnp.sum(retained * retained, axis=-1, keepdims=True) * (1.0 / DH)
                ret_all[at, cols] = (retained * lax.rsqrt(power + EPSILON)).astype(BF)
            return before + cum_row[b][:, SPAN - 1 : SPAN]

        first_half = cum_row[0][:, SPAN - 1 : SPAN]
        for b in range(1, half_blocks):
            first_half = first_half + cum_row[b][:, SPAN - 1 : SPAN]
        lax.fori_loop(0, half_blocks, step, first_half * which.astype(F32))

    across_half(other)
    ret_copy = pair_copy(ret_all, ret_in, 1)
    ret_copy.start()
    across_half(tp)
    l_wor.wait()

    def ret_own(n, _):
        total[:, tile_at(n)] += dot(ret_all[mine, :], w_ret[my_inputs, tile_at(n)])
        return 0

    lax.fori_loop(0, tiles, ret_own, 0)
    ret_copy.wait_recv()

    def out_copy(n):
        return pltpu.make_async_copy(
            out_vmem.at[:, tile_at(n)], out_hbm.at[:, tile_at(n)], out_sem.at[n]
        )

    def ret_other(n, _):
        final = total[:, tile_at(n)] + dot(ret_in[...], w_ret[other_inputs, tile_at(n)])
        out_vmem[:, tile_at(n)] = final.astype(BF)
        out_copy(n).start()
        return 0

    lax.fori_loop(0, tiles, ret_other, 0)

    for copy in tok_copies:
        copy.wait_send()
    for step in range(1, sp_count):
        @pl.when(sp + step < sp_count)
        def _():
            state_copy(step).wait_send()

    @pl.when(sp + 1 < sp_count)
    def _():
        rim_copy.wait_send()

    conv_copy.wait_send()
    ret_copy.wait_send()
    for n in range(tiles):
        out_copy(n).wait()


def rotation_tables(sp_count, rows):
    halfway = DH // 2
    inverse = 10000.0 ** (-np.arange(halfway, dtype=np.float64) / halfway)
    sign = np.concatenate([-np.ones(halfway), np.ones(halfway)])
    inverse = np.concatenate([inverse, inverse])

    def table(positions):
        angles = positions[:, None] * inverse[None, :]
        return np.stack([np.cos(angles), np.sin(angles) * sign]).astype(np.float32)

    inner = table(np.arange(SPAN))
    blocks = rows // SPAN
    outer = np.zeros((sp_count, 2, -(-blocks // 8) * 8, DH), np.float32)
    for device in range(sp_count):
        outer[device, :, :blocks] = table(SPAN * (device * blocks + np.arange(blocks)))
    return jnp.asarray(inner), jnp.asarray(outer)


def body(
    sp_count,
    tokens,
    norm_gain,
    w_query,
    w_key,
    w_value,
    log_decay,
    w_conv_in,
    w_conv_pre,
    w_conv_post,
    conv_taps,
    w_out_ret,
    w_out_conv,
):
    rows, half_width = tokens.shape
    width = 2 * half_width
    heads = log_decay.shape[0]
    local = heads * DH
    half = rows // 2
    blocks = rows // SPAN
    inner, outer = rotation_tables(sp_count, rows)
    any_spec = pl.BlockSpec(memory_space=pl.ANY)
    vmem, dma = pltpu.VMEM, pltpu.SemaphoreType.DMA
    scratch = [
        vmem((2, rows, half_width), BF),
        vmem((rows, width), BF),
        vmem((6, width, local), BF),
        vmem(w_out_ret.shape, BF),
        vmem(w_out_conv.shape, BF),
        vmem((1, width), BF),
        vmem(log_decay.shape, F32),
        vmem(conv_taps.shape, BF),
        vmem(inner.shape, F32),
        vmem(outer.shape[1:], F32),
        vmem((rows, DH), F32),
        vmem((rows, DH), F32),
        vmem((blocks, heads, SPAN), F32),
        vmem((rows, heads), F32),
        vmem((rows, heads), F32),
        vmem((rows, heads), F32),
        vmem((rows, local), BF),
        vmem((rows, local), BF),
        vmem((rows, local), BF),
        vmem((rows, local), BF),
        vmem((rows + 8, local), F32),
        vmem((blocks, local, DH), F32),
        vmem((local, DH), F32),
        vmem((local + 16 * heads, DH), BF),
        vmem((sp_count - 1, local + 16 * heads, DH), BF),
        vmem((local, DH), F32),
        vmem((rows, local), F32),
        vmem((rows, local), BF),
        vmem((half, local), BF),
        vmem((rows, local), BF),
        vmem((half, local), BF),
        vmem((half, width), F32),
        vmem((half, width), BF),
        dma((13,)),
        dma((2,)),
        dma((2,)),
        dma((2,)),
        dma((sp_count - 1,)),
        dma((sp_count - 1,)),
        dma((2,)),
        dma((2,)),
        dma,
        dma,
        dma((width // 512,)),
    ]
    return pl.pallas_call(
        functools.partial(kernel, sp_count),
        out_shape=jax.ShapeDtypeStruct((half, width), BF),
        in_specs=[any_spec] * 14,
        out_specs=any_spec,
        scratch_shapes=scratch,
        compiler_params=pltpu.CompilerParams(
            collective_id=0, has_side_effects=True, vmem_limit_bytes=60 * 1024 * 1024
        ),
        name="mixer",
    )(
        tokens,
        norm_gain.reshape(1, width),
        w_query,
        w_key,
        w_value,
        log_decay,
        w_conv_in,
        w_conv_pre,
        w_conv_post,
        conv_taps,
        w_out_ret,
        w_out_conv,
        inner,
        outer,
    )


def solution(mesh):
    in_specs = (
        P(("fs", "sp"), "tp"),
        P(),
        P(None, "tp"),
        P(None, "tp"),
        P(None, "tp"),
        P("tp", "sp"),
        P(None, "tp"),
        P(None, "tp"),
        P(None, "tp"),
        P(None, "tp"),
        P(),
        P(),
    )
    out_specs = P(("fs", "sp", "tp"), None)
    return jax.shard_map(
        functools.partial(body, mesh.shape["sp"]),
        mesh=mesh,
        in_specs=in_specs,
        out_specs=out_specs,
        check_vma=False,
    )
```

time: 142 us -> 43.6 us (0.31); the launches traced: 140 us -> 43.4 us
  Pallas kernels: 0 us -> 39.4 us
  matrix products: 34.4 us -> 0 us
  other arithmetic: 23.9 us -> 0 us
  local copies, waits for them, and re-layouts: 26.8 us -> 4.02 us
  blocking collectives: 19.3 us -> 0 us
  waiting for transfers between devices: 17.9 us -> 0 us
  between operations: 14.4 us -> 0.01 us
  starting transfers between devices: 3.32 us -> 0 us
    pallas_call x0 -> x1, Pallas kernels: none -> 39.4 us  [body(): pl.pallas_call(functools.partial(kernel, sp_count), out_shape=jax.ShapeDt...]
    dot_general x11 -> x0, matrix products: 34.4 us -> none  [the longest x6 17.8 us: project(): return jnp.dot(normed, weight, preferred_element_type=jnp.float32)]
    concatenate x8 -> x0, local copies, waits for them, and re-layouts: 19.3 us -> none  [rotate(): jnp.concatenate([leading * cosines - trailing * sinusoid, leading * sinus...]
    reduce_scatter x1 -> x0, waiting for transfers between devices: 16.5 us -> none  [body(): lax.psum_scatter((jnp.dot(ret_out, ret_rows, preferred_element_type=jnp.f...]
    all_gather x1 -> x0, blocking collectives: 12.3 us -> none  [body(): lax.all_gather(local_total[None].astype(jnp.bfloat16), 'sp', axis=0, tile...]
    unnamed x1 -> x0, blocking collectives: 6.95 us -> none
    add x6 -> x0, other arithmetic: 6.24 us -> none  [advance(): return (jnp.exp(end_decay)[:, None, None] * carried + fresh_state, carried)]
    convert_element_type x8 -> x0, other arithmetic: 4.48 us -> none  [the longest x1 2.35 us: body(): keys_turned = (rotate(project(w_key).reshape(tok_rows, head_count, DH), p...]
  transfers between devices with their start and end apart: 3 -> 0, of which waited for: 2 -> 0; matrix products, arithmetic and copies ran while one was open for 52% -> 0% of each run, Pallas kernels for 0% -> 0%
where the time goes in v1:
time: 43.6 us; the launch traced here: 43.4 us
  Pallas kernels  39.4 us (90%)
  local copies, waits for them, and re-layouts  4.02 us (9%)
    pallas_call x1, Pallas kernels, body(): pl.pallas_call(functools.partial(kernel, sp_count), out_shape=jax.ShapeDt...  39.4 us
    unnamed x1, local copies, waits for them, and re-layouts  2.73 us
    reshape x1, local copies, waits for them, and re-layouts, body(): norm_gain.reshape(1, width)  1.29 us

profile of v1, /device:TPU:21, one launch (start us, length us, event | category | flops | bytes accessed | tf_op | source)
XLA Modules:
  0.0 43.4 jit_solution(5208394472237380334)
XLA Ops:
  0.0 1.3 %reshape.3.gain_hbm = bf16[1,2048]{1,0:T(2,128)(2,1)} reshape(bf16[2048]{0:T(1024)(128)(2,1)} %param.15) | data formatting | bytes 8192 | tf_op jit(solution)/shard_map/reshape | solution.py:520
  1.3 39.4 %mixer.1 = bf16[384,2048]{1,0:T(8,128)(2,1)} custom-call(bf16[768,1024]{1,0:T(8,128)(2,1)} %tok_hbm.1, bf16[1,2048]{1,0:T(2,128)(2,1)} %reshape.3.gain_hbm, bf16[2048,512]{1,0:T(8,128)(2,1)} %wq_hbm.1, bf16[2048,512]{1,0:T(8,128)(2,1)} %wk_hbm.1, bf16[2048,512]{1,0:T(8,128)(2,1)} %wv_hbm.1, f32[4,768]{1,0:T(4,128)} %decay_hbm.1, bf16[2048,512]{1,0:T(8,128)(2,1)} %win_hbm.1, ...), custom_call_target="tpu_custom_call" | custom-call | tf_op jit(solution)/shard_map/mixer/pallas_call | solution.py:508
  40.7 2.7 %copy.16 = bf16[384,2048]{1,0:T(8,128)(2,1)} copy(bf16[384,2048]{1,0:T(8,128)(2,1)} %mixer.1) | data formatting | bytes 3145728

commit v2 on v1

--- a/solution.py
+++ b/solution.py
@@ -38,7 +38,7 @@
     woc_hbm,
     inner_hbm,
     outer_hbm,
-    out_hbm,
+    out_vmem,
     tok,
     normed,
     weights,
@@ -71,7 +71,6 @@
     ret_all,
     ret_in,
     total,
-    out_vmem,
     load_sem,
     tok_send,
     tok_recv,
@@ -82,7 +81,6 @@
     pair_recv,
     rim_send,
     rim_recv,
-    out_sem,
 ):
     rows, half_width = tok_hbm.shape
     width = 2 * half_width
@@ -173,6 +171,7 @@
         cum_col[at, :] = by_col
         exp_col[at, :] = jnp.exp(by_col)
         tail_col[at, :] = jnp.exp(by_col[SPAN - 1 : SPAN, :] - by_col)
+    gain_row = gain[...].astype(F32).reshape(1, width)
     running[...] = jnp.zeros_like(running)
     incoming[...] = jnp.zeros_like(incoming)
 
@@ -183,8 +182,8 @@
             x1 = tok[1, at, :].astype(F32)
             squares = jnp.sum(x0 * x0 + x1 * x1, axis=-1, keepdims=True)
             scale = lax.rsqrt(squares * (1.0 / width) + EPSILON)
-            normed[at, :half_width] = (x0 * scale * gain[:, :half_width].astype(F32)).astype(BF)
-            normed[at, half_width:] = (x1 * scale * gain[:, half_width:].astype(F32)).astype(BF)
+            normed[at, :half_width] = (x0 * scale * gain_row[:, :half_width]).astype(BF)
+            normed[at, half_width:] = (x1 * scale * gain_row[:, half_width:]).astype(BF)
             return 0
 
         lax.fori_loop(0, half // 32, step, 0)
@@ -387,15 +386,9 @@
     lax.fori_loop(0, tiles, ret_own, 0)
     ret_copy.wait_recv()
 
-    def out_copy(n):
-        return pltpu.make_async_copy(
-            out_vmem.at[:, tile_at(n)], out_hbm.at[:, tile_at(n)], out_sem.at[n]
-        )
-
     def ret_other(n, _):
         final = total[:, tile_at(n)] + dot(ret_in[...], w_ret[other_inputs, tile_at(n)])
         out_vmem[:, tile_at(n)] = final.astype(BF)
-        out_copy(n).start()
         return 0
 
     lax.fori_loop(0, tiles, ret_other, 0)
@@ -413,8 +406,6 @@
 
     conv_copy.wait_send()
     ret_copy.wait_send()
-    for n in range(tiles):
-        out_copy(n).wait()
 
 
 def rotation_tables(sp_count, rows):
@@ -457,7 +448,7 @@
     half = rows // 2
     blocks = rows // SPAN
     inner, outer = rotation_tables(sp_count, rows)
-    any_spec = pl.BlockSpec(memory_space=pl.ANY)
+    any_spec = pl.BlockSpec(memory_space=pltpu.HBM)
     vmem, dma = pltpu.VMEM, pltpu.SemaphoreType.DMA
     scratch = [
         vmem((2, rows, half_width), BF),
@@ -465,7 +456,7 @@
         vmem((6, width, local), BF),
         vmem(w_out_ret.shape, BF),
         vmem(w_out_conv.shape, BF),
-        vmem((1, width), BF),
+        vmem((width,), BF),
         vmem(log_decay.shape, F32),
         vmem(conv_taps.shape, BF),
         vmem(inner.shape, F32),
@@ -492,7 +483,6 @@
         vmem((rows, local), BF),
         vmem((half, local), BF),
         vmem((half, width), F32),
-        vmem((half, width), BF),
         dma((13,)),
         dma((2,)),
         dma((2,)),
@@ -503,21 +493,20 @@
         dma((2,)),
         dma,
         dma,
-        dma((width // 512,)),
     ]
     return pl.pallas_call(
         functools.partial(kernel, sp_count),
-        out_shape=jax.ShapeDtypeStruct((half, width), BF),
+        out_shape=pltpu.VMEM((half, width), BF),
         in_specs=[any_spec] * 14,
-        out_specs=any_spec,
+        out_specs=pl.BlockSpec(memory_space=pltpu.VMEM),
         scratch_shapes=scratch,
         compiler_params=pltpu.CompilerParams(
-            collective_id=0, has_side_effects=True, vmem_limit_bytes=60 * 1024 * 1024
+            collective_id=0, has_side_effects=True, vmem_limit_bytes=65400000
         ),
         name="mixer",
     )(
         tokens,
-        norm_gain.reshape(1, width),
+        norm_gain,
         w_query,
         w_key,
         w_value,

time: 43.6 us -> 39.9 us (0.915)
  local copies, waits for them, and re-layouts: 4.02 us -> 1.15 us
  Pallas kernels: 39.4 us -> 38.6 us
    unnamed x1, local copies, waits for them, and re-layouts: 2.73 us -> 1.15 us
    reshape x1 -> x0, local copies, waits for them, and re-layouts: 1.29 us -> none  [body(): norm_gain.reshape(1, width)]
    pallas_call x1, Pallas kernels: 39.4 us -> 38.6 us  [body(): pl.pallas_call(functools.partial(kernel, sp_count), out_shape=pltpu.VMEM(...]
where the time goes in v2:
time: 39.9 us; the launch traced here: 39.7 us
  Pallas kernels  38.6 us (97%)
  local copies, waits for them, and re-layouts  1.15 us (3%)
    pallas_call x1, Pallas kernels, body(): pl.pallas_call(functools.partial(kernel, sp_count), out_shape=pltpu.VMEM(...  38.6 us
    unnamed x1, local copies, waits for them, and re-layouts  1.15 us

profile of v2, /device:TPU:21, one launch (start us, length us, event | category | flops | bytes accessed | tf_op | source)
XLA Modules:
  0.0 39.7 jit_solution(15311072626922265601)
XLA Ops:
  0.0 38.6 %mixer.1 = bf16[384,2048]{1,0:T(8,128)(2,1)S(1)} custom-call(bf16[768,1024]{1,0:T(8,128)(2,1)} %tok_hbm.1, bf16[2048]{0:T(1024)(128)(2,1)} %gain_hbm.1, bf16[2048,512]{1,0:T(8,128)(2,1)} %wq_hbm.1, bf16[2048,512]{1,0:T(8,128)(2,1)} %wk_hbm.1, bf16[2048,512]{1,0:T(8,128)(2,1)} %wv_hbm.1, f32[4,768]{1,0:T(4,128)} %decay_hbm.1, bf16[2048,512]{1,0:T(8,128)(2,1)} %win_hbm.1, ...), custom_call_target="tpu_custom_call" | custom-call | tf_op jit(solution)/shard_map/mixer/pallas_call | solution.py:497
  38.6 1.1 %copy.16 = bf16[384,2048]{1,0:T(8,128)(2,1)} copy(bf16[384,2048]{1,0:T(8,128)(2,1)S(1)} %mixer.1) | data formatting | bytes 3145728
